TPU v7x, 32 devices: a whole 2x2x4 slice. The times are simulated.
32 devices in a mesh: ep: 8 (over z, y), tp: 4 (over x, core).
Axes of the slice: x: 2, y: 2, z: 4, core: 2. Of those that a mesh axis runs over, the one named last changes fastest.
Arguments:
- queries: bfloat16 [4096, 2048], P('ep', 'tp'), may hold values from -6 to 6
- forget_pre: float32 [4096, 2048], P('ep', 'tp'), may hold values from -8 to 20
- value_in: bfloat16 [4096, 2048], P('ep', 'tp'), may hold values from -6 to 6
- out_gate: bfloat16 [4096, 2048], P('ep', 'tp'), may hold values from -6 to 6
- lower_bound: float32 [2048], P('tp'), may hold values from 0.5 to 0.8
- out_gain: float32 [128], replicated, may hold values from 0.1 to 1.9
- out_weight: bfloat16 [2048, 2048], P('tp'), may hold values from -0.125 to 0.125
- moe_tokens: bfloat16 [2048, 2048], P('ep'), may hold values from -6 to 6
- moe_gain: float32 [2048], replicated, may hold values from 0.1 to 1.9
- expert_ids: int32 [2048, 4], P('ep'), may hold values from 0 to 15, all different within a row; in each aligned block of 64 rows (0 to 63, 64 to 127, ...) at most 32 rows name the same one
- route_weights: float32 [2048, 4], P('ep'), may hold values from 0.1 to 1
- w_gate: bfloat16 [16, 2048, 1024], P('ep', None, 'tp'), may hold values from -0.125 to 0.125
- w_up: bfloat16 [16, 2048, 1024], P('ep', None, 'tp'), may hold values from -0.125 to 0.125
- w_down: bfloat16 [16, 1024, 2048], P('ep', 'tp'), may hold values from -0.1875 to 0.1875
Outputs:
- mixer_out: bfloat16 [4096, 2048], P(('ep', 'tp'))
- expert_out: bfloat16 [2048, 2048], P(('ep', 'tp'))
Inputs may be any that keep to these rules, and one draw needn't show every extreme that they name: `expert_ids`: each row names 4 different experts. In each aligned block of 64 rows no expert is named by more than 32 rows, and in some block some expert is named by exactly 32 rows.
All inputs are finite; a program needn't handle non-finite values.
Results may differ from a plain program's by a relative error of at most 0.01065.
Values may be sent and summed in bfloat16 or wider, within the bound.
A program may use at most 128 MiB of HBM per device.

v0:
```python
import jax
import jax.numpy as jnp
from jax import lax
from jax.sharding import PartitionSpec as P

HEAD_DIM = 128
BLOCK = 64
EPS = 1e-06
HIGHEST = lax.Precision.HIGHEST


def prefix(part, axis, combine, identity):
    place = lax.axis_index(axis)
    gathered = jax.tree.map(lambda a: lax.all_gather(a, axis), part)
    state = jax.tree.map(lambda a, e: jnp.zeros_like(a) + jnp.asarray(e, a.dtype), part, identity)

    def one(hop, state):
        return combine(
            state, jax.tree.map(lambda a: lax.dynamic_index_in_dim(a, hop, 0, False), gathered)
        )

    return lax.fori_loop(0, place, one, state)


def rms_scale(values, gain):
    return values * lax.rsqrt(jnp.mean(values * values, axis=-1, keepdims=True) + EPS) * gain


def block_step(memory, inputs):
    queries_block, weight_block, values_block, forget_block = inputs
    cumulative = jnp.cumsum(forget_block, axis=1)
    length = queries_block.shape[1]
    causal = (
        jnp.arange(length, dtype=jnp.int32)[:, None] >= jnp.arange(length, dtype=jnp.int32)[None, :]
    )
    decayed_query = queries_block * jnp.exp(cumulative)
    decayed_key = weight_block * jnp.exp(-cumulative)
    carried_out = jnp.einsum("htd,hde->hte", decayed_query, memory, precision=HIGHEST)
    scores = jnp.einsum("htd,hsd->hts", decayed_query, decayed_key, precision=HIGHEST)
    scores = jnp.where(causal[None], scores, 0.0)
    local_out = jnp.einsum("hts,hse->hte", scores, values_block, precision=HIGHEST)
    block_total = cumulative[:, -1:, :]
    added = jnp.einsum(
        "hsd,hse->hde",
        weight_block * jnp.exp(block_total - cumulative),
        values_block,
        precision=HIGHEST,
    )
    memory = jnp.exp(block_total[:, 0, :])[:, :, None] * memory + added
    return (memory, carried_out + local_out)


def to_blocks(array, head_count):
    row_count = array.shape[0]
    return (
        array.astype(jnp.float32)
        .reshape(row_count // BLOCK, BLOCK, head_count, HEAD_DIM)
        .transpose(0, 2, 1, 3)
    )


def combine_memory(earlier, later):
    return (earlier[0] * later[0], later[0][:, :, None] * earlier[1] + later[1])


def slot_ranks(ids_block, expert_count):
    onehot = (
        ids_block[:, :, None] == jnp.arange(expert_count, dtype=jnp.int32)[None, None, :]
    ).astype(jnp.int32)
    return jnp.sum(onehot * (jnp.cumsum(onehot, axis=1) - 1), axis=2)


def local(
    queries,
    forget_pre,
    value_in,
    out_gate,
    lower_bound,
    out_gain,
    out_weight,
    moe_tokens,
    moe_gain,
    expert_ids,
    route_weights,
    w_gate,
    w_up,
    w_down,
):
    lanes = lax.axis_size("tp")
    lane_index = lax.axis_index("tp")
    ep_count = lax.axis_size("ep")
    seq_rows, local_width = queries.shape
    model_width = out_weight.shape[1]
    head_count = local_width // HEAD_DIM
    weight_in = (1.0 - lower_bound) * jax.nn.sigmoid(-forget_pre)
    log_forget = jnp.log1p(-weight_in)
    cumulative = jnp.cumsum(log_forget, axis=0)
    span_total = cumulative[-1]
    to_end = (weight_in * jnp.exp(span_total[None, :] - cumulative)).reshape(
        seq_rows, head_count, HEAD_DIM
    )
    values_float = value_in.astype(jnp.float32).reshape(seq_rows, head_count, HEAD_DIM)
    local_memory = jnp.einsum("shd,she->hde", to_end, values_float, precision=HIGHEST)
    decay_total = jnp.exp(span_total).reshape(head_count, HEAD_DIM)
    neutral = (jnp.ones_like(decay_total), jnp.zeros_like(local_memory))
    earlier_part = prefix((decay_total, local_memory), "ep", combine_memory, neutral)
    final_memory, outputs = lax.scan(
        block_step,
        earlier_part[1],
        (
            to_blocks(queries, head_count),
            to_blocks(weight_in, head_count),
            to_blocks(value_in, head_count),
            to_blocks(log_forget, head_count),
        ),
    )
    outputs = outputs.transpose(0, 2, 1, 3).reshape(seq_rows, head_count, HEAD_DIM)
    gate_act = jax.nn.silu(out_gate.astype(jnp.float32)).reshape(seq_rows, head_count, HEAD_DIM)
    gated = (
        (rms_scale(outputs, out_gain) * gate_act)
        .reshape(seq_rows, local_width)
        .astype(jnp.bfloat16)
    )
    qrows = moe_tokens.shape[0] // lanes
    top_count = expert_ids.shape[1]
    local_experts = w_gate.shape[0]
    expert_count = local_experts * ep_count
    capacity = max(2, 2 * qrows * top_count // expert_count)
    send_tokens = lax.dynamic_slice_in_dim(moe_tokens, lane_index * qrows, qrows, 0)
    send_ids = lax.dynamic_slice_in_dim(expert_ids, lane_index * qrows, qrows, 0)
    quarters = send_tokens.shape[0] // qrows
    normed = rms_scale(send_tokens.astype(jnp.float32), moe_gain).astype(jnp.bfloat16)
    ids_block = send_ids.reshape(quarters, qrows * top_count)
    ranks = slot_ranks(ids_block, expert_count)
    quarter_base = jnp.arange(quarters, dtype=jnp.int32)[:, None] * (expert_count * capacity)
    slot_index = (quarter_base + ids_block * capacity + ranks).reshape(-1)
    source_row = jnp.arange(quarters * qrows * top_count, dtype=jnp.int32) // top_count
    sources = (
        jnp.full((quarters * expert_count * capacity,), quarters * qrows, jnp.int32)
        .at[slot_index]
        .set(source_row)
    )
    padded = jnp.concatenate([normed, jnp.zeros((1, model_width), jnp.bfloat16)], axis=0)
    outgoing = padded[sources].reshape(quarters, ep_count, local_experts * capacity, model_width)
    arrived = lax.all_to_all(outgoing, "ep", split_axis=1, concat_axis=1, tiled=True)
    piece = lax.all_gather(arrived, "tp", axis=0, tiled=True)
    shaped = piece.reshape(piece.shape[0], ep_count, local_experts, capacity, model_width)
    gate_pre = jnp.einsum("qsecd,edf->qsecf", shaped, w_gate, preferred_element_type=jnp.float32)
    up_pre = jnp.einsum("qsecd,edf->qsecf", shaped, w_up, preferred_element_type=jnp.float32)
    hidden = (jax.nn.silu(gate_pre) * up_pre).astype(jnp.bfloat16)
    lane_rows = ep_count * local_experts * capacity
    mixer_sum = lax.psum_scatter(
        jnp.dot(gated, out_weight, preferred_element_type=jnp.float32).astype(jnp.bfloat16),
        "tp",
        scatter_dimension=0,
        tiled=True,
    )
    projected = jnp.einsum("qsecf,efd->qsecd", hidden, w_down, preferred_element_type=jnp.float32)
    expert_sum = lax.psum_scatter(
        projected.reshape(lax.axis_size("tp") * lane_rows, model_width).astype(jnp.bfloat16),
        "tp",
        scatter_dimension=0,
        tiled=True,
    )
    leaving = expert_sum.reshape(ep_count, local_experts * capacity, model_width)
    returned = lax.all_to_all(leaving, "ep", split_axis=0, concat_axis=0, tiled=True)
    returned = returned.reshape(expert_count * capacity, model_width)
    own_quarter = lane_index * (quarters // lanes)
    own_ids = lax.dynamic_index_in_dim(ids_block, own_quarter, 0, keepdims=False)
    own_ranks = lax.dynamic_index_in_dim(ranks, own_quarter, 0, keepdims=False)
    picked = (
        returned[own_ids * capacity + own_ranks]
        .astype(jnp.float32)
        .reshape(qrows, top_count, model_width)
    )
    own_weights = lax.dynamic_slice_in_dim(route_weights, lane_index * qrows, qrows, 0)
    expert_out = jnp.sum(picked * own_weights[:, :, None], axis=1).astype(jnp.bfloat16)
    return (mixer_sum, expert_out)


def solution(mesh):
    in_specs = (
        P("ep", "tp"),
        P("ep", "tp"),
        P("ep", "tp"),
        P("ep", "tp"),
        P("tp"),
        P(),
        P("tp", None),
        P("ep", None),
        P(),
        P("ep", None),
        P("ep", None),
        P("ep", None, "tp"),
        P("ep", None, "tp"),
        P("ep", "tp", None),
    )
    out_specs = (P(("ep", "tp"), None), P(("ep", "tp"), None))
    return jax.shard_map(local, mesh=mesh, in_specs=in_specs, out_specs=out_specs, check_vma=False)
```

profile of v0, /device:TPU:0, one launch (start us, length us, event | category | flops | bytes accessed | tf_op | source)
XLA Modules:
  0.0 324.8 jit_solution(6466362243241929309)
XLA Ops:
  9.6 1.4 scatter_custom_fusion
  13.3 3.3 %gather_fusion = bf16[512,2048]{1,0:T(8,128)(2,1)} fusion(bf16[65,2048]{1,0:T(8,128)(2,1)S(1)} %concatenate.3, s32[1024]{0:T(1024)S(1)} %pad_clamp_fusion.1), kind=kCustom, calls=%fused_computation | custom fusion | bytes 4196352 | tf_op jit(solution)/shard_map/gather | solution.py:144
  16.7 55.6 %all_to_all.10 = bf16[1,8,64,2048]{3,2,0,1:T(8,128)(2,1)} all-to-all(bf16[1,8,64,2048]{3,2,0,1:T(8,128)(2,1)} %bitcast.171), channel_id=1, replica_groups=mesh['ep'=8,'tp'=4] {'ep'}, dimensions={1} | all-to-all | bytes 4194304 | tf_op jit(solution)/shard_map/all_to_all | solution.py:145
  73.0 2.8 negate_log-plus-one_fusion
  77.5 1.5 broadcast_add_fusion
  80.6 2.6 copy.104
  83.3 2.8 fusion.40
  86.3 43.4 %all-gather.4.cloned.1.call-done = bf16[4,8,64,2048]{3,2,1,0:T(8,128)(2,1)} async-done(((bf16[1,8,64,2048]{3,2,1,0:T(8,128)(2,1)}), bf16[4,8,64,2048]{3,2,1,0:T(8,128)(2,1)}) %all-gather.4.cloned.1.call-update) | async-done | bytes 8388624 | tf_op jit(solution)/shard_map/all_gather | solution.py:146
  129.8 6.5 %fusion.15 = f32[2,4,8,32,256]{4,3,2,1,0:T(8,128)S(1)} fusion(bf16[4,8,2,32,2048]{4,3,2,1,0:T(8,128)(2,1)} %bitcast.199, bf16[2,2048,256]{2,1,0:T(8,128)(2,1)} %param.29), kind=kOutput, calls=%fused_computation.31 | convolution fusion | flops 2147483648 | bytes 12582912 | tf_op jit(solution)/shard_map/qsecd,edf->qsecf/dot_general | solution.py:148
  136.7 2.6 fusion.20
  139.4 5.6 %convert_bitcast_fusion = bf16[4,8,2,32,2048]{4,3,1,0,2:T(8,128)(2,1)} fusion(bf16[4,8,2,32,256]{4,3,1,0,2:T(8,128)(2,1)S(1)} %fusion.20, bf16[2,256,2048]{2,1,0:T(8,128)(2,1)S(1)} %copy-done), kind=kOutput, calls=%fused_computation.28 | convolution fusion | flops 2151677952 | bytes 11534336 | tf_op jit(solution)/shard_map/qsecf,efd->qsecd/dot_general | solution.py:158
  144.9 8.3 %copy.99 = bf16[4,8,2,32,2048]{4,3,2,1,0:T(8,128)(2,1)} copy(bf16[4,8,2,32,2048]{4,3,1,0,2:T(8,128)(2,1)} %convert_bitcast_fusion) | data formatting | bytes 16777216 | tf_op jit(solution)/shard_map/convert_element_type | solution.py:160
  153.3 1.3 reshape.281
  155.1 1.3 reshape.297
  156.4 2.4 reshape.298
  158.8 26.6 %all_gather.12 = f32[8,4,128]{2,1,0:T(4,128)S(1)} all-gather(f32[1,4,128]{2,1,0:T(4,128)S(1)} %bitcast.193), channel_id=1, replica_groups=mesh['ep'=8,'tp'=4] {'ep'}, dimensions={0}, use_global_device_ids=true | all-gather | bytes 18432 | tf_op jit(solution)/shard_map/all_gather | solution.py:14
  185.7 30.8 %while.25 = (s32[]{:T(128)}, f32[4,128,128]{2,1,0:T(8,128)S(1)}, f32[8,4,64,128]{3,2,1,0:T(8,128)S(1)}, f32[8,4,64,128]{3,1,2,0:T(4,128)}, f32[8,4,64,128]{3,1,2...) while((s32[]{:T(128)}, f32[4,128,128]{2,1,0:T(8,128)S(1)}, ...), condition=%wide.region_6.7_spmd, body=%wide.region_4.6_spmd.sunk | while | flops 153440256 | bytes 4083821 | solution.py:107
  218.4 4.3 %convolution_convert_fusion = bf16[512,2048]{1,0:T(8,128)(2,1)} fusion(bf16[512,2048]{1,0:T(8,128)(2,1)} %param.24, bf16[512,512]{1,0:T(8,128)(2,1)S(1)} %copy-done.11, f32[64,8,4,128]{3,2,1,0:T(4,128)S(1)} %bitcast.183, f32[64,8,4,128]{3,2,1,0:T(4,128)S(1)} %bitcast.185, f32[512]{0:T(512)S(1)} %broadcast_bitcast_fusion), kind=kOutput, calls=%fused_computation.33 | convolution fusion | flops 1077149696 | bytes 6817792 | tf_op jit(solution)/shard_map/dot_general | solution.py:153
  222.7 31.7 %reduce-scatter.5.cloned.1.call-done = bf16[512,2048]{1,0:T(8,128)(2,1)} async-done(((bf16[2048,2048]{1,0:T(8,128)(2,1)}), bf16[512,2048]{1,0:T(8,128)(2,1)}) %reduce-scatter.5.cloned.1.call-update) | async-done | bytes 2097168 | tf_op jit(solution)/shard_map/reduce_scatter | solution.py:159
  254.4 5.7 %all-to-all-start.1 = ((bf16[8,64,2048]{2,1,0:T(8,128)(2,1)}), bf16[8,64,2048]{2,1,0:T(8,128)(2,1)}, u32[]{:S(2)}, u32[]{:S(2)}) async-start(bf16[8,64,2048]{2,1,0:T(8,128)(2,1)} %bitcast.182), calls=%async_computation.3 | async-start | bytes 4194304 | tf_op jit(solution)/shard_map/all_to_all | solution.py:166
  260.2 48.0 %all-to-all-done.1 = bf16[8,64,2048]{2,1,0:T(8,128)(2,1)} async-done(((bf16[8,64,2048]{2,1,0:T(8,128)(2,1)}), bf16[8,64,2048]{2,1,0:T(8,128)(2,1)}, u32[]{:S(2)}, u32[]{:S(2)}) %all-to-all-start.1) | async-done | bytes 2097184 | tf_op jit(solution)/shard_map/all_to_all | solution.py:166
  308.2 4.4 %gather_fusion.1 = bf16[256,2048]{1,0:T(8,128)(2,1)S(1)} fusion(bf16[512,2048]{1,0:T(8,128)(2,1)} %bitcast.48, s32[1024]{0:T(1024)S(1)} %pad_clamp_fusion), kind=kCustom, calls=%fused_computation.1 | custom fusion | bytes 2098176 | tf_op jit(solution)/shard_map/gather | solution.py:172
  312.6 1.7 reshape.296
  314.3 3.9 %multiply_reduce_fusion = bf16[64,2048]{1,0:T(8,128)(2,1)} fusion(f32[64,4,2048]{2,1,0:T(4,128)} %reshape.296, f32[64,4]{1,0:T(8,128)S(1)} %copy.100), kind=kLoop, calls=%fused_computation.44 | loop fusion | flops 917504 | bytes 2360320 | tf_op jit(solution)/shard_map/reduce_sum | solution.py:177
  (167 shorter events, 42.2 us)
Async XLA Ops:
  7.2 132.2 %copy-start = (bf16[2,256,2048]{2,1,0:T(8,128)(2,1)S(1)}, bf16[2,256,2048]{2,1,0:T(8,128)(2,1)}, u32[]{:S(2)}) copy-start(bf16[2,256,2048]{2,1,0:T(8,128)(2,1)} %param.31) | copy-start | bytes 6291460
  7.2 122.6 %all-gather.4.cloned.1.call-start = ((), (), s32[]{:S(2)}) async-start(), calls=%async_computation.5 | async-start | bytes 10485760 | tf_op jit(solution)/shard_map/all_gather | solution.py:146
  72.3 0.7 copy-start.6
  72.4 113.1 %all-gather.6.cloned.1.call-start = ((), (), s32[]{:S(2)}) async-start(), calls=%async_computation.7 | async-start | bytes 2359296 | tf_op jit(solution)/shard_map/all_gather | solution.py:14
  76.5 1.0 copy-start.4
  77.5 1.9 copy-start.2
  86.1 168.3 %reduce-scatter.5.cloned.1.call-start = ((), (), s32[]{:S(2)}) async-start(), calls=%async_computation.6 | async-start | bytes 10485760 | tf_op jit(solution)/shard_map/reduce_scatter | solution.py:159
  129.8 6.5 %copy-start.9 = (bf16[4,8,64,2048]{3,2,1,0:T(8,128)(2,1)S(1)}, bf16[4,8,64,2048]{3,2,1,0:T(8,128)(2,1)}, u32[]{:S(2)}) copy-start(bf16[4,8,64,2048]{3,2,1,0:T(8,128)(2,1)} %all-gather.4.cloned.1.call-done) | copy-start | bytes 25165828
  129.8 7.0 %copy-start.10 = (bf16[2,2048,256]{2,1,0:T(8,128)(2,1)S(1)}, bf16[2,2048,256]{2,1,0:T(8,128)(2,1)}, u32[]{:S(2)}) copy-start(bf16[2,2048,256]{2,1,0:T(8,128)(2,1)} %param.30) | copy-start | bytes 6291460
  153.3 1.4 copy-start.3
  153.3 164.9 %reduce-scatter.3.cloned.1.call-start = ((), (), s32[]{:S(2)}) async-start(), calls=%async_computation.4 | async-start | bytes 2621440 | tf_op jit(solution)/shard_map/reduce_scatter | solution.py:152
  153.3 1.7 copy-start.5
  155.0 30.4 %copy-start.8 = (f32[128]{0:T(128)S(1)}, f32[128]{0:T(128)}, u32[]{:S(2)}) copy-start(f32[128]{0:T(128)} %param.23) | copy-start | bytes 1540
  216.9 1.5 copy-start.11
  254.4 5.7 %copy-start.7 = (f32[256,4]{0,1:T(4,128)S(1)}, f32[256,4]{0,1:T(4,128)}, u32[]{:S(2)}) copy-start(f32[256,4]{0,1:T(4,128)} %param.28) | copy-start | bytes 12292
  254.4 53.8 %all-to-all-start.1 = ((bf16[8,64,2048]{2,1,0:T(8,128)(2,1)}), bf16[8,64,2048]{2,1,0:T(8,128)(2,1)}, u32[]{:S(2)}, u32[]{:S(2)}) async-start(bf16[8,64,2048]{2,1,0:T(8,128)(2,1)} %bitcast.182), calls=%async_computation.3 | async-start | bytes 4194304 | tf_op jit(solution)/shard_map/all_to_all | solution.py:166
  308.2 10.0 %copy-start.1 = (bf16[2,256,2048]{2,1,0:T(8,128)(2,1)S(1)}, bf16[2,256,2048]{2,1,0:T(8,128)(2,1)}, u32[]{:S(2)}) copy-start(bf16[2,256,2048]{2,1,0:T(8,128)(2,1)} %param.31) | copy-start | bytes 6291460
Sparse Core Ops, SparseCore 0:
  72.5 57.2 all-gather.3
  132.5 49.1 all-gather.5
  184.3 70.0 reduce-scatter.4
  257.3 31.1 reduce-scatter.2
where the time goes:
time: 326 us; the launch traced here: 325 us
  waiting for transfers between devices  123 us (38%)
  blocking collectives  82.3 us (25%)
  local copies, waits for them, and re-layouts  47.9 us (15%)
  matrix products  34.9 us (11%)
  other arithmetic  15.5 us (5%)
  between operations  14.1 us (4%)
  starting transfers between devices  6 us (2%)
    all_to_all x1, blocking collectives, local(): lax.all_to_all(outgoing, 'ep', split_axis=1, concat_axis=1, tiled=True)  55.6 us
    all_to_all x1, waiting for transfers between devices, local(): lax.all_to_all(leaving, 'ep', split_axis=0, concat_axis=0, tiled=True)  48 us
    all_gather x1, waiting for transfers between devices, local(): piece = lax.all_gather(arrived, 'tp', axis=0, tiled=True)  43.4 us
    reduce_scatter x1, waiting for transfers between devices, local(): lax.psum_scatter(projected.reshape(lax.axis_size('tp') * lane_rows, model...  31.7 us
    all_gather x1, blocking collectives, prefix(): gathered = jax.tree.map(lambda a: lax.all_gather(a, axis), part)  26.6 us
    dynamic_slice x24, local copies, waits for them, and re-layouts, local(): lax.scan(block_step, earlier_part[1], (to_blocks(queries, head_count), to...  15.7 us
    convert_element_type x1, local copies, waits for them, and re-layouts, local(): projected.reshape(lax.axis_size('tp') * lane_rows, model_width)  8.31 us
  transfers between devices with their start and end apart: 5, of which 3 were waited for; matrix products, arithmetic and copies ran while one was open for 27% of the time, Pallas kernels for 0%

commit v1 on v0

--- a/solution.py
+++ b/solution.py
@@ -143,7 +143,12 @@
     padded = jnp.concatenate([normed, jnp.zeros((1, model_width), jnp.bfloat16)], axis=0)
     outgoing = padded[sources].reshape(quarters, ep_count, local_experts * capacity, model_width)
     arrived = lax.all_to_all(outgoing, "ep", split_axis=1, concat_axis=1, tiled=True)
-    piece = lax.all_gather(arrived, "tp", axis=0, tiled=True)
+    ring = [arrived]
+    for hop_ in range(3):
+        ring.append(lax.ppermute(ring[-1], "tp", [(dev, (dev + 1) % 4) for dev in range(4)]))
+    piece = jnp.roll(
+        jnp.concatenate(ring[::-1], axis=0), (lax.axis_index("tp") + 1) * ring[0].shape[0], axis=0
+    )
     shaped = piece.reshape(piece.shape[0], ep_count, local_experts, capacity, model_width)
     gate_pre = jnp.einsum("qsecd,edf->qsecf", shaped, w_gate, preferred_element_type=jnp.float32)
     up_pre = jnp.einsum("qsecd,edf->qsecf", shaped, w_up, preferred_element_type=jnp.float32)

time: 326 us -> 352 us (1.080)
  local copies, waits for them, and re-layouts: 47.9 us -> 79.6 us
  waiting for transfers between devices: 123 us -> 108 us
  starting transfers between devices: 6 us -> 10.9 us
    ppermute x0 -> x3, waiting for transfers between devices: none -> 64.9 us  [local(): lax.ppermute(ring[-1], 'tp', [(dev, (dev + 1) % 4) for dev in range(4)])]
    all_gather x1 -> x0, waiting for transfers between devices: 43.4 us -> none  [local(): piece = lax.all_gather(arrived, 'tp', axis=0, tiled=True)]
    reduce_scatter x1, waiting for transfers between devices: 31.7 us -> 0.03 us  [local(): lax.psum_scatter(projected.reshape(lax.axis_size('tp') * lane_rows, model...]
    unnamed x25 -> x46, local copies, waits for them, and re-layouts: 2.12 us -> 22.7 us
    dynamic_slice x0 -> x1, local copies, waits for them, and re-layouts: none -> 8.44 us  [local(): jnp.roll(jnp.concatenate(ring[::-1], axis=0), (lax.axis_index('tp') + 1)...]
    dot_general x8, matrix products: 2.95 us -> 8.23 us  [block_step(): jnp.einsum('htd,hde->hte', decayed_query, memory, precision=HIGHEST)]
    all_to_all x1, starting transfers between devices: 5.66 us -> 10.6 us  [local(): lax.all_to_all(leaving, 'ep', split_axis=0, concat_axis=0, tiled=True)]
    all_to_all x1, waiting for transfers between devices: 48 us -> 43.3 us  [local(): lax.all_to_all(leaving, 'ep', split_axis=0, concat_axis=0, tiled=True)]
  transfers between devices with their start and end apart: 5 -> 7, of which waited for: 3 -> 4; matrix products, arithmetic and copies ran while one was open for 27% -> 34% of each run, Pallas kernels for 0% -> 0%
where the time goes in v1:
time: 352 us; the launch traced here: 351 us
  waiting for transfers between devices  108 us (31%)
  blocking collectives  81.8 us (23%)
  local copies, waits for them, and re-layouts  79.6 us (23%)
  matrix products  37.9 us (11%)
  between operations  15.8 us (4%)
  other arithmetic  15.5 us (4%)
  starting transfers between devices  10.9 us (3%)
    ppermute x3, waiting for transfers between devices, local(): lax.ppermute(ring[-1], 'tp', [(dev, (dev + 1) % 4) for dev in range(4)])  64.9 us
    all_to_all x1, blocking collectives, local(): lax.all_to_all(outgoing, 'ep', split_axis=1, concat_axis=1, tiled=True)  55.7 us
    all_to_all x1, waiting for transfers between devices, local(): lax.all_to_all(leaving, 'ep', split_axis=0, concat_axis=0, tiled=True)  43.3 us
    all_gather x1, blocking collectives, prefix(): gathered = jax.tree.map(lambda a: lax.all_gather(a, axis), part)  26.1 us
    unnamed x46, local copies, waits for them, and re-layouts  22.7 us
    dynamic_slice x24, local copies, waits for them, and re-layouts, local(): lax.scan(block_step, earlier_part[1], (to_blocks(queries, head_count), to...  16 us
    all_to_all x1, starting transfers between devices, local(): lax.all_to_all(leaving, 'ep', split_axis=0, concat_axis=0, tiled=True)  10.6 us
    dynamic_slice x1, local copies, waits for them, and re-layouts, local(): jnp.roll(jnp.concatenate(ring[::-1], axis=0), (lax.axis_index('tp') + 1)...  8.44 us
  transfers between devices with their start and end apart: 7, of which 4 were waited for; matrix products, arithmetic and copies ran while one was open for 34% of the time, Pallas kernels for 0%

profile of v1, /device:TPU:0, one launch (start us, length us, event | category | flops | bytes accessed | tf_op | source)
XLA Modules:
  0.0 350.5 jit_solution(16510293347616376082)
XLA Ops:
  14.2 3.3 gather_fusion
  17.5 55.7 %all_to_all.10 = bf16[1,8,64,2048]{3,2,0,1:T(8,128)(2,1)S(1)} all-to-all(bf16[1,8,64,2048]{3,2,0,1:T(8,128)(2,1)} %bitcast.178), channel_id=1, replica_groups=mesh['ep'=8,'tp'=4] {'ep'}, dimensions={1} | all-to-all | bytes 4194304 | tf_op jit(solution)/shard_map/all_to_all | solution.py:145
  74.5 25.5 %collective-permute-done = bf16[1,8,64,2048]{3,2,1,0:T(8,128)(2,1)S(1)} collective-permute-done((bf16[1,8,64,2048]{3,2,1,0:T(8,128)(2,1)S(1)}, bf16[1,8,64,2048]{3,2,1,0:T(8,128)(2,1)S(1)}, u32[]{:S(2)}, u32[]{:S(2)}) %collective-permute-start) | collective-permute-done | bytes 2097184 | tf_op jit(solution)/shard_map/ppermute | solution.py:148
  101.3 25.6 %collective-permute-done.1 = bf16[1,8,64,2048]{3,2,1,0:T(8,128)(2,1)} collective-permute-done((bf16[1,8,64,2048]{3,2,1,0:T(8,128)(2,1)S(1)}, bf16[1,8,64,2048]{3,2,1,0:T(8,128)(2,1)}, u32[]{:S(2)}, u32[]{:S(2)}) %collective-permute-start.1) | collective-permute-done | bytes 2097184 | tf_op jit(solution)/shard_map/ppermute | solution.py:148
  133.3 2.5 copy.110
  135.8 2.7 fusion.40
  138.8 13.9 %collective-permute-done.2 = bf16[1,8,64,2048]{3,2,1,0:T(8,128)(2,1)} collective-permute-done((bf16[1,8,64,2048]{3,2,1,0:T(8,128)(2,1)}, bf16[1,8,64,2048]{3,2,1,0:T(8,128)(2,1)}, u32[]{:S(2)}, u32[]{:S(2)}) %collective-permute-start.2) | collective-permute-done | bytes 2097184 | tf_op jit(solution)/shard_map/ppermute | solution.py:148
  152.6 3.2 constant_dynamic-update-slice_fusion.7
  155.8 3.3 constant_dynamic-update-slice_fusion.6
  163.0 3.2 constant_dynamic-update-slice_fusion.3
  166.2 3.1 constant_dynamic-update-slice_fusion.2
  172.2 8.4 %constant_dynamic-slice_fusion.5 = bf16[4,8,64,2048]{3,2,1,0:T(8,128)(2,1)} fusion(bf16[8,8,64,2048]{3,2,1,0:T(8,128)(2,1)} %constant_dynamic-update-slice_fusion, s32[]{:T(128)S(6)} %select_n.57), kind=kLoop, calls=%fused_computation.102 | loop fusion | bytes 16777220 | tf_op jit(solution)/shard_map/jit(_roll_dynamic)/dynamic_slice | solution.py:149
  180.7 5.9 %fusion.15 = f32[2,4,8,32,256]{4,3,2,1,0:T(8,128)S(1)} fusion(bf16[4,8,2,32,2048]{4,3,2,1,0:T(8,128)(2,1)} %bitcast.176, bf16[2,2048,256]{2,1,0:T(8,128)(2,1)S(1)} %copy-done.15), kind=kOutput, calls=%fused_computation.31 | convolution fusion | flops 2147483648 | bytes 12582912 | tf_op jit(solution)/shard_map/qsecd,edf->qsecf/dot_general | solution.py:153
  187.0 2.6 fusion.20
  189.7 5.6 %convert_bitcast_fusion = bf16[4,8,2,32,2048]{4,3,1,0,2:T(8,128)(2,1)} fusion(bf16[4,8,2,32,256]{4,3,1,0,2:T(8,128)(2,1)S(1)} %fusion.20, bf16[2,256,2048]{2,1,0:T(8,128)(2,1)S(1)} %copy-done), kind=kOutput, calls=%fused_computation.28 | convolution fusion | flops 2151677952 | bytes 11534336 | tf_op jit(solution)/shard_map/qsecf,efd->qsecd/dot_general | solution.py:163
  195.3 8.3 %copy.105 = bf16[4,8,2,32,2048]{4,3,2,1,0:T(8,128)(2,1)} copy(bf16[4,8,2,32,2048]{4,3,1,0,2:T(8,128)(2,1)} %convert_bitcast_fusion) | data formatting | bytes 16777216 | tf_op jit(solution)/shard_map/convert_element_type | solution.py:165
  204.9 2.6 reshape.282
  210.2 26.1 %all_gather.9 = f32[8,4,128]{2,1,0:T(4,128)S(1)} all-gather(f32[1,4,128]{2,1,0:T(4,128)S(1)} %bitcast.197), channel_id=1, replica_groups=mesh['ep'=8,'tp'=4] {'ep'}, dimensions={0}, use_global_device_ids=true | all-gather | bytes 18432 | tf_op jit(solution)/shard_map/all_gather | solution.py:14
  236.6 36.3 %while.25 = (s32[]{:T(128)}, f32[4,128,128]{2,1,0:T(8,128)S(1)}, f32[8,4,64,128]{3,2,1,0:T(8,128)}, f32[8,4,64,128]{3,1,2,0:T(4,128)}, f32[8,4,64,128]{3,1,2,0:T...) while((s32[]{:T(128)}, f32[4,128,128]{2,1,0:T(8,128)S(1)}, ...), condition=%wide.region_6.7_spmd, body=%wide.region_4.6_spmd.sunk | while | flops 153440256 | bytes 4084329 | solution.py:107
  276.4 2.7 convolution_convert_fusion
  279.2 10.6 %all-to-all-start.1 = ((bf16[8,64,2048]{2,1,0:T(8,128)(2,1)}), bf16[8,64,2048]{2,1,0:T(8,128)(2,1)}, u32[]{:S(2)}, u32[]{:S(2)}) async-start(bf16[8,64,2048]{2,1,0:T(8,128)(2,1)} %bitcast.186), calls=%async_computation.3 | async-start | bytes 4194304 | tf_op jit(solution)/shard_map/all_to_all | solution.py:171
  289.9 43.3 %all-to-all-done.1 = bf16[8,64,2048]{2,1,0:T(8,128)(2,1)} async-done(((bf16[8,64,2048]{2,1,0:T(8,128)(2,1)}), bf16[8,64,2048]{2,1,0:T(8,128)(2,1)}, u32[]{:S(2)}, u32[]{:S(2)}) %all-to-all-start.1) | async-done | bytes 2097184 | tf_op jit(solution)/shard_map/all_to_all | solution.py:171
  333.3 4.2 %gather_fusion.1 = bf16[256,2048]{1,0:T(8,128)(2,1)S(1)} fusion(bf16[512,2048]{1,0:T(8,128)(2,1)} %bitcast.50, s32[1024]{0:T(1024)S(1)} %pad_clamp_fusion), kind=kCustom, calls=%fused_computation.1 | custom fusion | bytes 2098176 | tf_op jit(solution)/shard_map/gather | solution.py:177
  339.2 3.9 %multiply_reduce_fusion = bf16[64,2048]{1,0:T(8,128)(2,1)} fusion(f32[64,4,2048]{2,1,0:T(4,128)} %reshape.296, f32[64,4]{1,0:T(8,128)S(1)} %copy.106), kind=kLoop, calls=%fused_computation.44 | loop fusion | flops 917504 | bytes 2360320 | tf_op jit(solution)/shard_map/reduce_sum | solution.py:182
  (193 shorter events, 68.1 us)
Async XLA Ops:
  8.0 181.7 %copy-start = (bf16[2,256,2048]{2,1,0:T(8,128)(2,1)S(1)}, bf16[2,256,2048]{2,1,0:T(8,128)(2,1)}, u32[]{:S(2)}) copy-start(bf16[2,256,2048]{2,1,0:T(8,128)(2,1)} %param.31) | copy-start | bytes 6291460
  8.0 228.3 %all-gather.3.cloned.1.call-start = ((), (), s32[]{:S(2)}) async-start(), calls=%async_computation.6 | async-start | bytes 2359296 | tf_op jit(solution)/shard_map/all_gather | solution.py:14
  17.5 109.4 %copy-start.12 = (f32[512]{0:T(512)S(1)}, f32[512]{0:T(512)}, u32[]{:S(2)}) copy-start(f32[512]{0:T(512)} %param.22) | copy-start | bytes 6148
  17.5 109.4 %copy-start.10 = (f32[512,512]{1,0:T(8,128)S(1)}, f32[512,512]{1,0:T(8,128)}, u32[]{:S(2)}) copy-start(f32[512,512]{1,0:T(8,128)} %param.19) | copy-start | bytes 3145732
  74.5 25.5 %collective-permute-start = (bf16[1,8,64,2048]{3,2,1,0:T(8,128)(2,1)S(1)}, bf16[1,8,64,2048]{3,2,1,0:T(8,128)(2,1)S(1)}, u32[]{:S(2)}, u32[]{:S(2)}) collective-permute-start(bf16[1,8,64,2048]{3,2,1,0:T(8,128)(2,1)S(1)} %bitcast.173), channel_id=1, source_target_pairs={{0,1},{1,2},{2,3},{3,0},{4,5},{5,6},{6,7},{7,4},{8,9},{9,10},{10,1... | collective-permute-start | bytes 6291464 | tf_op jit(solution)/shard_map/ppermute | solution.py:148
  100.0 1.3 copy-start.5
  101.3 25.6 %collective-permute-start.1 = (bf16[1,8,64,2048]{3,2,1,0:T(8,128)(2,1)S(1)}, bf16[1,8,64,2048]{3,2,1,0:T(8,128)(2,1)}, u32[]{:S(2)}, u32[]{:S(2)}) collective-permute-start(bf16[1,8,64,2048]{3,2,1,0:T(8,128)(2,1)S(1)} %collective-permute-done), channel_id=1, source_target_pairs={{0,1},{1,2},{2,3},{3,0},{4,5},{5,6},{6,7},{7,4},{8,9},{9,10},{10,1... | collective-permute-start | bytes 6291464 | tf_op jit(solution)/shard_map/ppermute | solution.py:148
  126.9 25.8 %collective-permute-start.2 = (bf16[1,8,64,2048]{3,2,1,0:T(8,128)(2,1)}, bf16[1,8,64,2048]{3,2,1,0:T(8,128)(2,1)}, u32[]{:S(2)}, u32[]{:S(2)}) collective-permute-start(bf16[1,8,64,2048]{3,2,1,0:T(8,128)(2,1)} %collective-permute-done.1), channel_id=1, source_target_pairs={{0,1},{1,2},{2,3},{3,0},{4,5},{5,6},{6,7},{7,4},{8,9},{9,10},{10,1... | collective-permute-start | bytes 6291464 | tf_op jit(solution)/shard_map/ppermute | solution.py:148
  130.2 1.8 copy-start.3
  138.5 140.6 %reduce-scatter.5.cloned.1.call-start = ((), (), s32[]{:S(2)}) async-start(), calls=%async_computation.5 | async-start | bytes 10485760 | tf_op jit(solution)/shard_map/reduce_scatter | solution.py:164
  155.8 3.3 copy-start.6
  159.1 2.3 copy-start.2
  172.2 8.4 %copy-start.15 = (bf16[2,2048,256]{2,1,0:T(8,128)(2,1)S(1)}, bf16[2,2048,256]{2,1,0:T(8,128)(2,1)}, u32[]{:S(2)}) copy-start(bf16[2,2048,256]{2,1,0:T(8,128)(2,1)} %param.29) | copy-start | bytes 6291460
  180.7 5.9 %copy-start.4 = (bf16[4,8,64,2048]{3,2,1,0:T(8,128)(2,1)S(1)}, bf16[4,8,64,2048]{3,2,1,0:T(8,128)(2,1)}, u32[]{:S(2)}) copy-start(bf16[4,8,64,2048]{3,2,1,0:T(8,128)(2,1)} %constant_dynamic-slice_fusion.5) | copy-start | bytes 25165828
  180.7 6.4 %copy-start.16 = (bf16[2,2048,256]{2,1,0:T(8,128)(2,1)S(1)}, bf16[2,2048,256]{2,1,0:T(8,128)(2,1)}, u32[]{:S(2)}) copy-start(bf16[2,2048,256]{2,1,0:T(8,128)(2,1)} %param.30) | copy-start | bytes 6291460
  203.6 139.5 %reduce-scatter.3.cloned.1.call-start = ((), (), s32[]{:S(2)}) async-start(), calls=%async_computation.4 | async-start | bytes 2621440 | tf_op jit(solution)/shard_map/reduce_scatter | solution.py:157
  204.9 2.6 copy-start.9
  204.9 4.0 %copy-start.11 = (bf16[512,512]{1,0:T(8,128)(2,1)S(1)}, bf16[512,512]{1,0:T(8,128)(2,1)}, u32[]{:S(2)}) copy-start(bf16[512,512]{1,0:T(8,128)(2,1)} %param.18) | copy-start | bytes 1572868
  207.6 28.8 %copy-start.14 = (f32[128]{0:T(128)S(1)}, f32[128]{0:T(128)}, u32[]{:S(2)}) copy-start(f32[128]{0:T(128)} %param.23) | copy-start | bytes 1540
  272.9 1.9 copy-start.8
  274.7 1.6 copy-start.17
  274.7 1.7 copy-start.18
  279.1 10.6 %copy-start.13 = (f32[256,4]{0,1:T(4,128)S(1)}, f32[256,4]{0,1:T(4,128)}, u32[]{:S(2)}) copy-start(f32[256,4]{0,1:T(4,128)} %param.28) | copy-start | bytes 12292
  279.2 54.1 %all-to-all-start.1 = ((bf16[8,64,2048]{2,1,0:T(8,128)(2,1)}), bf16[8,64,2048]{2,1,0:T(8,128)(2,1)}, u32[]{:S(2)}, u32[]{:S(2)}) async-start(bf16[8,64,2048]{2,1,0:T(8,128)(2,1)} %bitcast.186), calls=%async_computation.3 | async-start | bytes 4194304 | tf_op jit(solution)/shard_map/all_to_all | solution.py:171
  (2 other events, 2.4 us)
Sparse Core Ops, SparseCore 0:
  138.6 48.4 all-gather.2
Sparse Core Ops, SparseCore 1:
  203.7 70.5 reduce-scatter.4
  279.2 37.1 reduce-scatter.2
